TPU v7x, 32 devices: a whole 2x2x4 slice. The times are simulated.
32 devices in a mesh: rep: 2 (over x), fs: 8 (over z, y), tp: 2 (over core).
Axes of the slice: x: 2, y: 2, z: 4, core: 2. Of those that a mesh axis runs over, the one named last changes fastest.
Arguments:
- tokens: bfloat16 [6144, 2048], P(('rep', 'fs', 'tp')), may hold values from -6 to 6
- mix_gain_in: float32 [2048], replicated, may hold values from 0.1 to 1.9
- pool_weight: bfloat16 [4, 512, 512], P(None, 'fs'), may hold values from -0.25 to 0.25
- mix_gain_out: float32 [2048], replicated, may hold values from 0.1 to 1.9
- ffn_gain_in: float32 [2048], replicated, may hold values from 0.1 to 1.9
- gate_weight: bfloat16 [2048, 5632], P('fs', 'tp'), may hold values from -0.125 to 0.125
- up_weight: bfloat16 [2048, 5632], P('fs', 'tp'), may hold values from -0.125 to 0.125
- gate_taps: float32 [3, 5632], replicated, may hold values from -3.5 to 3.5
- up_taps: float32 [3, 5632], replicated, may hold values from -3.5 to 3.5
- down_weight: bfloat16 [5632, 2048], P('tp', 'fs'), may hold values from -0.078125 to 0.078125
- ffn_gain_out: float32 [2048], replicated, may hold values from 0.1 to 1.9
Outputs:
- mixed_out: bfloat16 [6144, 2048], P(('rep', 'fs', 'tp'))
All inputs are finite; a program needn't handle non-finite values.
Results may differ from a plain program's by a relative error of at most 0.014.
Values may be sent and summed in bfloat16 or wider, within the bound.
A program may use at most 128 MiB of HBM per device.

v0:
```python
import jax
import jax.numpy as jnp
from jax import lax
from jax.sharding import PartitionSpec as P

pool_spans = (2, 4, 8, 16)
rms_eps = 1e-06


def rms_scale(values, gain):
    floats = values.astype(jnp.float32)
    return floats * lax.rsqrt(jnp.mean(floats * floats, axis=-1, keepdims=True) + rms_eps) * gain


def pooled_gap(padded, count):
    margin = padded.shape[0] - count
    floats = padded.astype(jnp.float32)
    width = padded.shape[1] // len(pool_spans)
    where = jnp.arange(count, dtype=jnp.int32)
    pieces = []
    for group, span in enumerate(pool_spans):
        block = floats[:, group * width : (group + 1) * width]
        total = jnp.zeros((count, width), jnp.float32)
        for back in range(span):
            total = total + block[margin - back : margin - back + count]
        divisor = jnp.minimum(where + 1, span).astype(jnp.float32)
        pieces.append(total / divisor[:, None] - block[margin:])
    return jnp.concatenate(pieces, axis=1).astype(jnp.bfloat16)


def mix_groups(gap, pool_full):
    length, features = gap.shape
    groups = pool_full.shape[0]
    shaped = gap.reshape(length, groups, features // groups)
    result = jnp.einsum("rgc,gcj->rgj", shaped, pool_full, preferred_element_type=jnp.float32)
    return result.reshape(length, features).astype(jnp.bfloat16)


def causal_taps(pre, taps):
    width = taps.shape[0]
    floats = pre.astype(jnp.float32)
    padded = jnp.concatenate([jnp.zeros((width - 1, pre.shape[1]), jnp.float32), floats], axis=0)
    total = jnp.zeros(floats.shape, jnp.float32)
    for offset in range(width):
        total = total + taps[offset] * padded[offset : offset + pre.shape[0]]
    return total


def shards(
    tokens,
    mix_gain_in,
    pool_weight,
    mix_gain_out,
    ffn_gain_in,
    gate_weight,
    up_weight,
    gate_taps,
    up_taps,
    down_weight,
    ffn_gain_out,
):
    rows, features = tokens.shape
    margin = max(pool_spans) - 1
    position = lax.axis_index("tp")
    pool_full = lax.all_gather(pool_weight, "fs", axis=1, tiled=True)
    every = lax.all_gather(tokens, "tp", axis=0, tiled=True)
    length = every.shape[0]
    normed = rms_scale(every, mix_gain_in).astype(jnp.bfloat16)
    padded = jnp.concatenate([jnp.zeros((margin, features), jnp.bfloat16), normed], axis=0)
    gap = pooled_gap(padded, length)
    mixed = mix_groups(gap, pool_full)
    after_all = every.astype(jnp.float32) + rms_scale(mixed, mix_gain_out)
    whole = rms_scale(after_all, ffn_gain_in).astype(jnp.bfloat16)
    after_mix = lax.dynamic_slice_in_dim(after_all, position * rows, rows, 0)
    columns = gate_weight.shape[1]
    gate_part = jnp.dot(
        whole,
        lax.all_gather(gate_weight, "fs", axis=0, tiled=True),
        preferred_element_type=jnp.float32,
    )
    up_part = jnp.dot(
        whole,
        lax.all_gather(up_weight, "fs", axis=0, tiled=True),
        preferred_element_type=jnp.float32,
    )
    offset = position * columns
    gate_local = lax.dynamic_slice_in_dim(gate_taps, offset, columns, 1)
    up_local = lax.dynamic_slice_in_dim(up_taps, offset, columns, 1)
    gate_conv = causal_taps(gate_part.astype(jnp.bfloat16), gate_local)
    up_conv = causal_taps(up_part.astype(jnp.bfloat16), up_local)
    hidden = (jax.nn.gelu(gate_conv, approximate=True) * up_conv).astype(jnp.bfloat16)
    down_full = lax.all_gather(down_weight, "fs", axis=1, tiled=True)
    channel_out = lax.psum_scatter(
        jnp.dot(hidden, down_full, preferred_element_type=jnp.float32).astype(jnp.bfloat16),
        "tp",
        scatter_dimension=0,
        tiled=True,
    ).astype(jnp.float32)
    return (after_mix + rms_scale(channel_out, ffn_gain_out)).astype(jnp.bfloat16)


def solution(mesh):
    in_specs = (
        P(("rep", "fs", "tp"), None),
        P(),
        P(None, "fs", None),
        P(),
        P(),
        P("fs", "tp"),
        P("fs", "tp"),
        P(),
        P(),
        P("tp", "fs"),
        P(),
    )
    out_specs = P(("rep", "fs", "tp"), None)
    return jax.shard_map(shards, mesh=mesh, in_specs=in_specs, out_specs=out_specs, check_vma=False)
```

profile of v0, /device:TPU:0, one launch (start us, length us, event | category | flops | bytes accessed | tf_op | source)
XLA Modules:
  0.0 600.9 jit_solution(8342491924516857888)
XLA Ops:
  6.5 0.7 all-gather.6.cloned.1.call-update
  7.3 0.0 all-gather.8.cloned.1.call-start
  7.3 0.7 all-gather.8.cloned.1.call-update
  8.0 0.0 all-gather.10.cloned.1.call-start
  8.1 0.7 all-gather.10.cloned.1.call-update
  8.8 0.0 all-gather.12.cloned.1.call-start
  8.8 0.5 all-gather.12.cloned.1.call-update
  9.3 0.0 all-gather.14.cloned.1.call-start
  9.4 0.5 all-gather.14.cloned.1.call-update
  9.9 0.0 reduce-scatter.2.cloned.1.call-start
  10.0 1.2 dynamic-slice_reduce_fusion.2
  11.2 10.2 %all-gather.6.cloned.1.call-done = bf16[384,2048]{1,0:T(8,128)(2,1)} async-done(((bf16[192,2048]{1,0:T(8,128)(2,1)}), bf16[384,2048]{1,0:T(8,128)(2,1)}) %all-gather.6.cloned.1.call-update) | async-done | bytes 1572880 | tf_op jit(solution)/shard_map/all_gather | solution.py:66
  21.4 1.8 fusion.12
  23.2 1.8 fusion.14
  25.1 0.5 pad_convert_fusion
  25.5 1.0 fusion.51
  26.5 1.2 fusion.48
  27.7 46.2 %all-gather.8.cloned.1.call-done = bf16[4,512,512]{2,1,0:T(8,128)(2,1)} async-done(((bf16[4,64,512]{2,1,0:T(8,128)(2,1)}), bf16[4,512,512]{2,1,0:T(8,128)(2,1)}) %all-gather.8.cloned.1.call-update) | async-done | bytes 2097168 | tf_op jit(solution)/shard_map/all_gather | solution.py:65
  73.9 2.7 fusion.11
  76.6 0.4 convert_bitcast_fusion
  77.0 0.3 copy.13
  77.3 1.1 copy-done
  78.4 0.8 multiply_reduce_fusion
  79.2 158.8 %all-gather.10.cloned.1.call-done = bf16[2048,2816]{1,0:T(8,128)(2,1)} async-done(((bf16[256,2816]{1,0:T(8,128)(2,1)}), bf16[2048,2816]{1,0:T(8,128)(2,1)}) %all-gather.10.cloned.1.call-update) | async-done | bytes 11534352 | tf_op jit(solution)/shard_map/all_gather | solution.py:78
  238.0 9.7 %fusion.10 = f32[384,2816]{1,0:T(8,128)} fusion(bf16[2048,2816]{1,0:T(8,128)(2,1)} %all-gather.10.cloned.1.call-done, f32[384,2048]{1,0:T(8,128)S(1)} %get-tuple-element.12, f32[2048]{0:T(1024)S(1)} %copy-done.4, f32[384]{0:T(512)S(1)} %add_rsqrt_fusion), kind=kOutput, calls=%fused_computation.16 | convolution fusion | flops 4433707008 | bytes 19015168 | tf_op jit(solution)/shard_map/dot_general | solution.py:76
  247.6 153.9 %all-gather.12.cloned.1.call-done = bf16[2048,2816]{1,0:T(8,128)(2,1)} async-done(((bf16[256,2816]{1,0:T(8,128)(2,1)}), bf16[2048,2816]{1,0:T(8,128)(2,1)}) %all-gather.12.cloned.1.call-update) | async-done | bytes 11534352 | tf_op jit(solution)/shard_map/all_gather | solution.py:83
  401.5 9.6 %fusion.9 = f32[384,2816]{1,0:T(8,128)} fusion(bf16[2048,2816]{1,0:T(8,128)(2,1)} %all-gather.12.cloned.1.call-done, f32[384,2048]{1,0:T(8,128)S(1)} %get-tuple-element.12, f32[2048]{0:T(1024)S(1)} %copy-done.4, f32[384]{0:T(512)S(1)} %add_rsqrt_fusion), kind=kOutput, calls=%fused_computation.14 | convolution fusion | flops 4433707008 | bytes 19015168 | tf_op jit(solution)/shard_map/dot_general | solution.py:81
  411.1 153.8 %all-gather.14.cloned.1.call-done = bf16[2816,2048]{1,0:T(8,128)(2,1)} async-done(((bf16[2816,256]{1,0:T(8,128)(2,1)}), bf16[2816,2048]{1,0:T(8,128)(2,1)}) %all-gather.14.cloned.1.call-update) | async-done | bytes 11534352 | tf_op jit(solution)/shard_map/all_gather | solution.py:92
  565.0 18.0 %convolution_convert_fusion.2 = bf16[384,2048]{1,0:T(8,128)(2,1)} fusion(bf16[2816,2048]{1,0:T(8,128)(2,1)} %all-gather.14.cloned.1.call-done, f32[384,2816]{1,0:T(8,128)} %fusion.9, f32[384,2816]{1,0:T(8,128)} %fusion.10, f32[2816]{0:T(1024)S(1)} %get-tuple-element.10, f32[2816]{0:T(1024)S(1)} %get-tuple-element.9, f32[2816]{0:T(1024)S(1)} %get-tuple-element.8, ...), kind=kOutput, calls=%fused_computation.25 | convolution fusion | flops 4451598336 | bytes 21825536 | tf_op jit(solution)/shard_map/dot_general | solution.py:94
  583.0 7.4 %reduce-scatter.2.cloned.1.call-done = bf16[192,2048]{1,0:T(8,128)(2,1)} async-done(((bf16[384,2048]{1,0:T(8,128)(2,1)}), bf16[192,2048]{1,0:T(8,128)(2,1)}) %reduce-scatter.2.cloned.1.call-update) | async-done | bytes 786448 | tf_op jit(solution)/shard_map/reduce_scatter | solution.py:93
  590.3 1.4 fusion.25
  591.7 2.3 fusion.28
  (18 shorter events, 0.1 us)
Async XLA Ops:
  6.5 14.9 %all-gather.6.cloned.1.call-start = ((), (), s32[]{:S(2)}) async-start(), calls=%async_computation.1 | async-start | bytes 2359296 | tf_op jit(solution)/shard_map/all_gather | solution.py:66
  7.3 16.0 %copy-start.1 = (f32[2048]{0:T(1024)S(1)}, f32[2048]{0:T(1024)}, u32[]{:S(2)}) copy-start(f32[2048]{0:T(1024)} %param.12) | copy-start | bytes 24580
  7.3 66.6 %all-gather.8.cloned.1.call-start = ((), (), s32[]{:S(2)}) async-start(), calls=%async_computation.2 | async-start | bytes 2359296 | tf_op jit(solution)/shard_map/all_gather | solution.py:65
  8.0 229.9 %all-gather.10.cloned.1.call-start = ((), (), s32[]{:S(2)}) async-start(), calls=%async_computation.3 | async-start | bytes 12976128 | tf_op jit(solution)/shard_map/all_gather | solution.py:78
  8.8 392.8 %all-gather.12.cloned.1.call-start = ((), (), s32[]{:S(2)}) async-start(), calls=%async_computation.4 | async-start | bytes 12976128 | tf_op jit(solution)/shard_map/all_gather | solution.py:83
  9.3 555.6 %all-gather.14.cloned.1.call-start = ((), (), s32[]{:S(2)}) async-start(), calls=%async_computation.5 | async-start | bytes 12976128 | tf_op jit(solution)/shard_map/all_gather | solution.py:92
  9.9 580.4 %reduce-scatter.2.cloned.1.call-start = ((), (), s32[]{:S(2)}) async-start(), calls=%async_computation.6 | async-start | bytes 2359296 | tf_op jit(solution)/shard_map/reduce_scatter | solution.py:93
  77.0 1.4 copy-start
  77.0 1.4 copy-start.3
  78.4 159.6 %copy-start.4 = (f32[2048]{0:T(1024)S(1)}, f32[2048]{0:T(1024)}, u32[]{:S(2)}) copy-start(f32[2048]{0:T(1024)} %param.15) | copy-start | bytes 24580
  565.0 26.8 %copy-start.2 = (f32[2048]{0:T(1024)S(1)}, f32[2048]{0:T(1024)}, u32[]{:S(2)}) copy-start(f32[2048]{0:T(1024)} %param.21) | copy-start | bytes 24580
Sparse Core Ops, SparseCore 0:
  8.9 12.5 all-gather.5
  23.6 50.2 all-gather.7
  76.1 161.8 all-gather.9
  240.0 161.4 all-gather.11
  403.4 161.4 all-gather.13
  583.1 7.2 reduce-scatter.1
where the time goes:
time: 601 us
  waiting for transfers between devices  533 us (89%)
  matrix products  39.9 us (7%)
  between operations  13.6 us (2%)
  other arithmetic  11.2 us (2%)
    all_gather x1, waiting for transfers between devices, shards(): lax.all_gather(gate_weight, 'fs', axis=0, tiled=True)  159 us
    all_gather x1, waiting for transfers between devices, shards(): lax.all_gather(up_weight, 'fs', axis=0, tiled=True)  154 us
    all_gather x1, waiting for transfers between devices, shards(): down_full = lax.all_gather(down_weight, 'fs', axis=1, tiled=True)  154 us
    all_gather x1, waiting for transfers between devices, shards(): pool_full = lax.all_gather(pool_weight, 'fs', axis=1, tiled=True)  46.2 us
    dot_general x1, matrix products, shards(): jnp.dot(hidden, down_full, preferred_element_type=jnp.float32)  18 us
  transfers between devices with their start and end apart: 6, of which 6 were waited for; matrix products, arithmetic and copies ran while one was open for 5% of the time, Pallas kernels for 0%

commit v1 on v0

--- a/solution.py
+++ b/solution.py
@@ -89,7 +89,7 @@
     gate_conv = causal_taps(gate_part.astype(jnp.bfloat16), gate_local)
     up_conv = causal_taps(up_part.astype(jnp.bfloat16), up_local)
     hidden = (jax.nn.gelu(gate_conv, approximate=True) * up_conv).astype(jnp.bfloat16)
-    down_full = lax.all_gather(down_weight, "fs", axis=1, tiled=True)
+    down_full = jnp.concatenate(lax.all_gather(down_weight, "fs"), axis=1)
     channel_out = lax.psum_scatter(
         jnp.dot(hidden, down_full, preferred_element_type=jnp.float32).astype(jnp.bfloat16),
         "tp",

time: 601 us -> 611 us (1.017)
  local copies, waits for them, and re-layouts: 2.58 us -> 18 us
    reshape x0 -> x1, local copies, waits for them, and re-layouts: none -> 15.4 us  [shards(): down_full = jnp.concatenate(lax.all_gather(down_weight, 'fs'), axis=1)]
  transfers between devices with their start and end apart: 6 -> 6, of which waited for: 6 -> 6; matrix products, arithmetic and copies ran while one was open for 5% -> 6% of each run, Pallas kernels for 0% -> 0%
where the time goes in v1:
time: 611 us; the launch traced here: 610 us
  waiting for transfers between devices  528 us (86%)
  matrix products  39.7 us (6%)
  local copies, waits for them, and re-layouts  18 us (3%)
  between operations  13.6 us (2%)
  other arithmetic  11.2 us (2%)
    all_gather x1, waiting for transfers between devices, shards(): down_full = jnp.concatenate(lax.all_gather(down_weight, 'fs'), axis=1)  159 us
    all_gather x1, waiting for transfers between devices, shards(): lax.all_gather(gate_weight, 'fs', axis=0, tiled=True)  154 us
    all_gather x1, waiting for transfers between devices, shards(): lax.all_gather(up_weight, 'fs', axis=0, tiled=True)  148 us
    all_gather x1, waiting for transfers between devices, shards(): pool_full = lax.all_gather(pool_weight, 'fs', axis=1, tiled=True)  46.2 us
    dot_general x1, matrix products, shards(): jnp.dot(hidden, down_full, preferred_element_type=jnp.float32)  17.7 us
    reshape x1, local copies, waits for them, and re-layouts, shards(): down_full = jnp.concatenate(lax.all_gather(down_weight, 'fs'), axis=1)  15.4 us
  transfers between devices with their start and end apart: 6, of which 6 were waited for; matrix products, arithmetic and copies ran while one was open for 6% of the time, Pallas kernels for 0%

profile of v1, /device:TPU:0, one launch (start us, length us, event | category | flops | bytes accessed | tf_op | source)
XLA Modules:
  0.0 610.4 jit_solution(12383845677126318486)
XLA Ops:
  6.5 0.7 all-gather.7.cloned.1.call-update
  7.3 0.7 all-gather.9.cloned.1.call-update
  8.0 0.0 all-gather.15.cloned.1.call-start
  8.1 0.7 all-gather.15.cloned.1.call-update
  8.8 0.0 all-gather.13.cloned.1.call-start
  8.8 0.5 all-gather.13.cloned.1.call-update
  9.3 0.0 all-gather.11.cloned.1.call-start
  9.4 0.5 all-gather.11.cloned.1.call-update
  9.9 0.0 reduce-scatter.2.cloned.1.call-start
  10.0 1.2 dynamic-slice_reduce_fusion.2
  11.2 10.2 %all-gather.7.cloned.1.call-done = bf16[384,2048]{1,0:T(8,128)(2,1)} async-done(((bf16[192,2048]{1,0:T(8,128)(2,1)}), bf16[384,2048]{1,0:T(8,128)(2,1)}) %all-gather.7.cloned.1.call-update) | async-done | bytes 1572880 | tf_op jit(solution)/shard_map/all_gather | solution.py:66
  21.4 1.8 fusion.12
  23.2 1.8 fusion.14
  25.1 0.5 pad_convert_fusion
  25.5 1.0 fusion.51
  26.5 1.2 fusion.48
  27.7 46.2 %all-gather.9.cloned.1.call-done = bf16[4,512,512]{2,1,0:T(8,128)(2,1)} async-done(((bf16[4,64,512]{2,1,0:T(8,128)(2,1)}), bf16[4,512,512]{2,1,0:T(8,128)(2,1)}) %all-gather.9.cloned.1.call-update) | async-done | bytes 2097168 | tf_op jit(solution)/shard_map/all_gather | solution.py:65
  73.9 2.7 fusion.11
  76.5 0.4 convert_bitcast_fusion
  77.0 0.3 copy.16
  77.3 1.1 copy-done
  78.4 0.8 multiply_reduce_fusion
  79.2 158.8 %all-gather.15.cloned.1.call-done = bf16[22528,256]{1,0:T(8,128)(2,1)} async-done(((bf16[2816,256]{1,0:T(8,128)(2,1)}), bf16[22528,256]{1,0:T(8,128)(2,1)}) %all-gather.15.cloned.1.call-update) | async-done | bytes 11534352 | tf_op jit(solution)/shard_map/all_gather | solution.py:92
  238.0 15.4 %copy.15 = bf16[2816,8,256]{0,2,1:T(8,128)(2,1)} copy(bf16[2816,8,256]{2,0,1:T(8,128)(2,1)} %bitcast.21) | data formatting | bytes 23068672 | tf_op jit(solution)/shard_map/reshape | solution.py:92
  253.4 148.2 %all-gather.13.cloned.1.call-done = bf16[2048,2816]{1,0:T(8,128)(2,1)} async-done(((bf16[256,2816]{1,0:T(8,128)(2,1)}), bf16[2048,2816]{1,0:T(8,128)(2,1)}) %all-gather.13.cloned.1.call-update) | async-done | bytes 11534352 | tf_op jit(solution)/shard_map/all_gather | solution.py:83
  401.5 9.7 %fusion.9 = f32[384,2816]{1,0:T(8,128)} fusion(bf16[2048,2816]{1,0:T(8,128)(2,1)} %all-gather.13.cloned.1.call-done, f32[384,2048]{1,0:T(8,128)S(1)} %get-tuple-element.12, f32[2048]{0:T(1024)S(1)} %copy-done.4, f32[384]{0:T(512)S(1)} %add_rsqrt_fusion), kind=kOutput, calls=%fused_computation.14 | convolution fusion | flops 4433707008 | bytes 19015168 | tf_op jit(solution)/shard_map/dot_general | solution.py:81
  411.2 153.9 %all-gather.11.cloned.1.call-done = bf16[2048,2816]{1,0:T(8,128)(2,1)} async-done(((bf16[256,2816]{1,0:T(8,128)(2,1)}), bf16[2048,2816]{1,0:T(8,128)(2,1)}) %all-gather.11.cloned.1.call-update) | async-done | bytes 11534352 | tf_op jit(solution)/shard_map/all_gather | solution.py:78
  565.1 9.7 %fusion.10 = f32[384,2816]{1,0:T(8,128)} fusion(bf16[2048,2816]{1,0:T(8,128)(2,1)} %all-gather.11.cloned.1.call-done, f32[384,2048]{1,0:T(8,128)S(1)} %get-tuple-element.12, f32[2048]{0:T(1024)S(1)} %copy-done.4, f32[384]{0:T(512)S(1)} %add_rsqrt_fusion), kind=kOutput, calls=%fused_computation.16 | convolution fusion | flops 4433707008 | bytes 19015168 | tf_op jit(solution)/shard_map/dot_general | solution.py:76
  574.8 17.7 %convolution_convert_fusion.2 = bf16[384,2048]{1,0:T(8,128)(2,1)} fusion(bf16[2816,2048]{0,1:T(8,128)(2,1)} %bitcast.22, f32[384,2816]{1,0:T(8,128)} %fusion.9, f32[384,2816]{1,0:T(8,128)} %fusion.10, f32[2816]{0:T(1024)S(1)} %get-tuple-element.10, f32[2816]{0:T(1024)S(1)} %get-tuple-element.9, f32[2816]{0:T(1024)S(1)} %get-tuple-element.8, ...), kind=kOutput, calls=%fused_computation.25 | convolution fusion | flops 4451598336 | bytes 21825536 | tf_op jit(solution)/shard_map/dot_general | solution.py:94
  592.5 7.4 %reduce-scatter.2.cloned.1.call-done = bf16[192,2048]{1,0:T(8,128)(2,1)} async-done(((bf16[384,2048]{1,0:T(8,128)(2,1)}), bf16[192,2048]{1,0:T(8,128)(2,1)}) %reduce-scatter.2.cloned.1.call-update) | async-done | bytes 786448 | tf_op jit(solution)/shard_map/reduce_scatter | solution.py:93
  599.9 1.4 fusion.25
  601.2 2.3 fusion.28
  (19 shorter events, 0.1 us)
Async XLA Ops:
  6.5 14.9 %all-gather.7.cloned.1.call-start = ((), (), s32[]{:S(2)}) async-start(), calls=%async_computation.1 | async-start | bytes 2359296 | tf_op jit(solution)/shard_map/all_gather | solution.py:66
  7.3 16.0 %copy-start.1 = (f32[2048]{0:T(1024)S(1)}, f32[2048]{0:T(1024)}, u32[]{:S(2)}) copy-start(f32[2048]{0:T(1024)} %param.12) | copy-start | bytes 24580
  7.3 66.6 %all-gather.9.cloned.1.call-start = ((), (), s32[]{:S(2)}) async-start(), calls=%async_computation.2 | async-start | bytes 2359296 | tf_op jit(solution)/shard_map/all_gather | solution.py:65
  8.0 229.9 %all-gather.15.cloned.1.call-start = ((), (), s32[]{:S(2)}) async-start(), calls=%async_computation.6 | async-start | bytes 12976128 | tf_op jit(solution)/shard_map/all_gather | solution.py:92
  8.8 392.8 %all-gather.13.cloned.1.call-start = ((), (), s32[]{:S(2)}) async-start(), calls=%async_computation.4 | async-start | bytes 12976128 | tf_op jit(solution)/shard_map/all_gather | solution.py:83
  9.3 555.8 %all-gather.11.cloned.1.call-start = ((), (), s32[]{:S(2)}) async-start(), calls=%async_computation.3 | async-start | bytes 12976128 | tf_op jit(solution)/shard_map/all_gather | solution.py:78
  9.9 589.9 %reduce-scatter.2.cloned.1.call-start = ((), (), s32[]{:S(2)}) async-start(), calls=%async_computation.5 | async-start | bytes 2359296 | tf_op jit(solution)/shard_map/reduce_scatter | solution.py:93
  77.0 1.4 copy-start
  77.0 1.4 copy-start.3
  238.0 163.6 %copy-start.4 = (f32[2048]{0:T(1024)S(1)}, f32[2048]{0:T(1024)}, u32[]{:S(2)}) copy-start(f32[2048]{0:T(1024)} %param.15) | copy-start | bytes 24580
  574.8 26.5 %copy-start.2 = (f32[2048]{0:T(1024)S(1)}, f32[2048]{0:T(1024)}, u32[]{:S(2)}) copy-start(f32[2048]{0:T(1024)} %param.21) | copy-start | bytes 24580
Sparse Core Ops, SparseCore 0:
  8.9 12.5 all-gather.6
  23.6 50.2 all-gather.8
  76.1 161.8 all-gather.14
  240.0 161.4 all-gather.12
  403.6 161.4 all-gather.10
  592.6 7.2 reduce-scatter.1
